TPU v7x, 32 devices: a whole 2x2x4 slice. The times are simulated.
32 devices in a mesh: dp: 4 (over y, x), kv: 4 (over z), tp: 2 (over core).
Axes of the slice: x: 2, y: 2, z: 4, core: 2. Of those that a mesh axis runs over, the one named last changes fastest.
Arguments:
- tokens: bfloat16 [32, 4, 2048], P('dp', None, 'kv'), may hold values from -600 to 600
- input_norm_gain: float32 [2048], P('kv'), may hold values from 0.1 to 1.9
- query_projection: bfloat16 [2048, 1024], P('kv', 'tp'), may hold values from -0.125 to 0.125
- key_projection: bfloat16 [2048, 1024], P('kv', 'tp'), may hold values from -0.125 to 0.125
- value_projection: bfloat16 [2048, 1024], P('kv', 'tp'), may hold values from -0.125 to 0.125
- write_strength_weight: bfloat16 [2048, 16], P('kv', 'tp'), may hold values from -0.125 to 0.125
- decay_projection: bfloat16 [2048, 16], P('kv', 'tp'), may hold values from -0.125 to 0.125
- head_decay_rate: float32 [16], P('tp'), may hold values from 0.02 to 0.6
- token_extra_decay: float32 [32, 4, 16], P(('dp', 'kv'), None, 'tp'), may hold values from -0.7 to 0
- accepted: int32 [32], P(('dp', 'kv')), may hold values from 1 to 4
- prior_step_states: float32 [32, 4, 16, 4096], P(('dp', 'kv'), None, 'tp'), may hold values from -4 to 4
- output_norm_gain: float32 [64], replicated, may hold values from 0.1 to 1.9
- output_projection: bfloat16 [1024, 2048], P('tp', 'kv'), may hold values from -0.1875 to 0.1875
Outputs:
- mixed: bfloat16 [32, 4, 2048], P('dp', None, 'kv')
- updated_states: float32 [32, 4, 16, 4096], P(('dp', 'kv'), None, 'tp')
Inputs may be any that keep to these rules, and one draw needn't show every extreme that they name: `accepted`: how many proposals of the previous step each sequence kept; its state after that many is taken up.
All inputs are finite; a program needn't handle non-finite values.
Results may differ from a plain program's by a relative error of at most 0.029.
Values may be sent and summed in bfloat16 or wider, within the bound.
A program may use at most 64 MiB of HBM per device.

v0:
```python
import functools
import jax
import jax.numpy as jnp
from jax import lax
from jax.experimental import pallas as pl
from jax.experimental.pallas import tpu as pltpu
from jax.sharding import PartitionSpec as P

epsilon = 1e-06
MESH = pl.DeviceIdType.MESH
f32 = jnp.float32
bf16 = jnp.bfloat16
LANES = 128
VMEM_LIMIT = 32 * 2 ** 20


def far_first(n):
    return sorted(range(1, n), key=lambda o: (abs(2 * o - n), o))


def near_first(n):
    return sorted(range(1, n), key=lambda o: (-abs(2 * o - n), o))


def silu(u):
    return u / (1.0 + jnp.exp(-u))


def kernel(
    n,
    ntp,
    head_size,
    tokens_hbm,
    gain_hbm,
    wq_hbm,
    wk_hbm,
    wv_hbm,
    wb_hbm,
    wd_hbm,
    rate_hbm,
    extra_hbm,
    accepted_hbm,
    prior_hbm,
    onorm_hbm,
    wo_hbm,
    mixed_ref,
    states_v,
    tokens_v,
    gain_v,
    w_v,
    wb_v,
    wd_v,
    rate_v,
    extra_v,
    accepted_s,
    prior_v,
    onorm_v,
    wo_v,
    x_v,
    part_v,
    aux_v,
    send_v,
    recv_v,
    recva_v,
    heads_v,
    gates_v,
    spread_v,
    expand_v,
    att_v,
    flat_v,
    normed_v,
    recvn_v,
    outp_v,
    recvp_v,
    load_sem,
    rs_send,
    rs_recv,
    ag_send,
    ag_recv,
    tp_send,
    tp_recv,
):
    me = lax.axis_index("kv")
    my_tp = lax.axis_index("tp")
    group_seqs, steps, feature_dev = tokens_v.shape
    own_seqs, _, heads, state_len = prior_v.shape
    own_rows = own_seqs * steps
    model_width = n * feature_dev

    barrier = pltpu.get_barrier_semaphore()
    for o in far_first(n):
        pl.semaphore_signal(
            barrier, inc=1, device_id={"kv": lax.rem(me + o, n)}, device_id_type=MESH
        )
    for o in range(1, ntp):
        pl.semaphore_signal(
            barrier, inc=1, device_id={"tp": lax.rem(my_tp + o, ntp)}, device_id_type=MESH
        )

    loads = {}
    for index, (name, source, target) in enumerate((
        ("tokens", tokens_hbm, tokens_v),
        ("gain", gain_hbm, gain_v),
        ("wb", wb_hbm, wb_v),
        ("wd", wd_hbm, wd_v),
        ("q", wq_hbm, w_v.at[0]),
        ("k", wk_hbm, w_v.at[1]),
        ("v", wv_hbm, w_v.at[2]),
        ("prior", prior_hbm, prior_v),
        ("rate", rate_hbm, rate_v),
        ("extra", extra_hbm, extra_v),
        ("accepted", accepted_hbm, accepted_s),
        ("onorm", onorm_hbm, onorm_v),
        ("wo", wo_hbm, wo_v),
    )):
        loads[name] = pltpu.make_async_copy(source, target, load_sem.at[index])
        loads[name].start()

    loads["tokens"].wait()
    loads["gain"].wait()
    for s in range(group_seqs):
        x_v[s * steps:(s + 1) * steps, :] = tokens_v[s].astype(f32)
    x = x_v[...]
    squares = jnp.sum(x * x, axis=1, keepdims=True)
    scaled = (x * gain_v[...]).astype(bf16)

    contract_last = (((1,), (1,)), ((), ()))
    loads["wb"].wait()
    loads["wd"].wait()
    beta_part = lax.dot_general(scaled, wb_v[...], contract_last, preferred_element_type=f32)
    decay_part = lax.dot_general(scaled, wd_v[...], contract_last, preferred_element_type=f32)
    lane = lax.broadcasted_iota(jnp.int32, (x.shape[0], LANES), 1)
    aux_v[...] = jnp.where(lane == 2 * heads, squares, 0.0).reshape(aux_v.shape)
    aux_v[:, :, 0:heads] = beta_part.reshape(n, own_rows, heads)
    aux_v[:, :, heads:2 * heads] = decay_part.reshape(n, own_rows, heads)

    def project_in(piece, name):
        loads[name].wait()
        part = jnp.dot(scaled, w_v[piece], preferred_element_type=f32)
        part = part.reshape(n, own_rows, part.shape[1])
        part_v[piece] = part
        send_v[:, piece] = part.astype(bf16)

    project_in(0, "q")
    pl.semaphore_wait(barrier, n - 1 + ntp - 1)

    sends = []
    rs = {}

    def remote(source, target, send_sem, recv_sem, device):
        copy = pltpu.make_async_remote_copy(
            src_ref=source,
            dst_ref=target,
            send_sem=send_sem,
            recv_sem=recv_sem,
            device_id=device,
            device_id_type=MESH,
        )
        copy.start()
        sends.append(copy)
        return copy

    for o in far_first(n):
        target = lax.rem(me + o, n)
        rs[3, o] = remote(
            aux_v.at[target], recva_v.at[o - 1], rs_send.at[3, o - 1], rs_recv.at[3, o - 1],
            {"kv": target},
        )
    for piece, span in ((0, pl.ds(0, 1)), (1, pl.ds(1, 2))):
        if piece > 0:
            project_in(1, "k")
            project_in(2, "v")
        for o in far_first(n):
            target = lax.rem(me + o, n)
            rs[piece, o] = remote(
                send_v.at[target, span], recv_v.at[o - 1, span],
                rs_send.at[piece, o - 1], rs_recv.at[piece, o - 1], {"kv": target},
            )

    entry = lax.broadcasted_iota(jnp.int32, spread_v.shape, 0)
    column = lax.broadcasted_iota(jnp.int32, spread_v.shape, 1)
    first = jnp.where(entry < head_size, entry, entry - head_size) * head_size
    spread_v[...] = jnp.where(
        (column >= first) & (column < first + head_size), 1.0, 0.0
    ).astype(bf16)

    for name in ("rate", "extra", "accepted", "onorm", "prior"):
        loads[name].wait()

    aux = aux_v[me]
    for o in near_first(n):
        rs[3, o].wait_recv()
        aux = aux + recva_v[o - 1]
    inverse = lax.rsqrt(aux[:, 2 * heads:2 * heads + 1] / model_width + epsilon)
    pre = aux * inverse
    beta_pre = pre[:, 0:heads]
    decay_pre = pre[:, heads:2 * heads]
    softplus = jnp.maximum(decay_pre, 0.0) + jnp.log1p(jnp.exp(-jnp.abs(decay_pre)))
    extra = jnp.concatenate([extra_v[s] for s in range(own_seqs)], axis=0)
    gates_v[...] = jnp.zeros(gates_v.shape, f32)
    gates_v[:, 0:heads] = 1.0 / (1.0 + jnp.exp(-beta_pre))
    gates_v[:, heads:2 * heads] = jnp.exp(-rate_v[...] * softplus + extra)
    gates = gates_v[...].T

    def summed(piece):
        total = part_v[piece, me]
        for o in near_first(n):
            if piece < 2:
                rs[piece, o].wait_recv()
            total = total + recv_v[o - 1, piece].astype(f32)
        value = silu(total * inverse)
        for h in range(heads):
            heads_v[piece, :, h, :] = value[:, h * head_size:(h + 1) * head_size]
        return heads_v[piece]

    def unit(value):
        return value * lax.rsqrt(jnp.sum(value * value, axis=-1, keepdims=True) + epsilon)

    tall = own_rows * heads
    for piece, scale in ((0, head_size ** -0.5), (1, 1.0)):
        value = (unit(summed(piece)) * scale).reshape(tall, head_size)
        high = value.astype(bf16)
        low = (value - high.astype(f32)).astype(bf16)
        both = jnp.concatenate([high.astype(f32), low.astype(f32)], axis=1).astype(bf16)
        expand_v[piece] = jnp.dot(both, spread_v[...], preferred_element_type=f32)
    value_heads = summed(2)

    def fold(product):
        width = product.shape[1]
        while width > LANES:
            width //= 2
            product = product[:, :width] + product[:, width:]
        return product + pltpu.roll(product, head_size, 1)

    current = [
        prior_v[s, jnp.clip(accepted_s[s] - 1, 0, steps - 1)] for s in range(own_seqs)
    ]
    for t in range(steps):
        for s in range(own_seqs):
            state = current[s]
            row = s * steps + t
            block = pl.ds(row * heads, heads)
            key_wide = expand_v[1, block, :]
            beta = gates[0:heads, row:row + 1]
            decay = gates[heads:2 * heads, row:row + 1]
            value = value_heads[row]
            value = jnp.concatenate([value] * (LANES // head_size), axis=1)
            write = beta * (value - decay * fold(key_wide * state))
            write = jnp.concatenate([write] * (state_len // LANES), axis=1)
            state = decay * state + key_wide * write
            states_v[s, t] = state
            current[s] = state
            attended = fold(expand_v[0, block, :] * state)
            att_v[row] = attended[:, 0:head_size]

    attended = att_v[...]
    mean = jnp.sum(attended * attended, axis=-1, keepdims=True) / head_size
    att_v[...] = attended * lax.rsqrt(mean + epsilon) * onorm_v[...].reshape(1, 1, head_size)
    for h in range(heads):
        flat_v[:, h * head_size:(h + 1) * head_size] = att_v[:, h, :]
    normed = flat_v[...].astype(bf16)
    normed_v[...] = normed

    gather = {}
    for o in far_first(n):
        gather[o] = remote(
            normed_v, recvn_v.at[o - 1], ag_send.at[o - 1], ag_recv.at[o - 1],
            {"kv": lax.rem(me + o, n)},
        )
    loads["wo"].wait()
    exchange = {}

    def project(o, rows):
        outp_v[o] = jnp.dot(rows, wo_v[...], preferred_element_type=f32).astype(bf16)
        for p in range(1, ntp):
            exchange[o, p] = remote(
                outp_v.at[o], recvp_v.at[p - 1, o], tp_send.at[p - 1, o], tp_recv.at[p - 1, o],
                {"tp": lax.rem(my_tp + p, ntp)},
            )

    order = [0] + near_first(n)
    project(0, normed)
    for o in near_first(n):
        gather[o].wait_recv()
        project(o, recvn_v[o - 1])
    for o in order:
        total = outp_v[o].astype(f32)
        for p in range(1, ntp):
            exchange[o, p].wait_recv()
            total = total + recvp_v[p - 1, o].astype(f32)
        source = lax.rem(me - o + n, n) * own_seqs
        for s in range(own_seqs):
            mixed_ref[source + s] = total[s * steps:(s + 1) * steps].astype(bf16)

    for copy in sends:
        copy.wait_send()


def finish(mixed_v, states_v, mixed_hbm, states_hbm, sem):
    own_seqs, steps = states_v.shape[:2]
    copies = [
        pltpu.make_async_copy(
            states_v.at[s, t], states_hbm.at[s, t], sem.at[1 + s * steps + t]
        )
        for s in range(own_seqs)
        for t in range(steps)
    ]
    copies.append(pltpu.make_async_copy(mixed_v, mixed_hbm, sem.at[0]))
    for copy in copies:
        copy.start()
    for copy in copies:
        copy.wait()


def per_device(n, ntp, *args):
    (
        tokens, input_norm_gain, query_projection, key_projection, value_projection,
        write_strength_weight, decay_projection, head_decay_rate, token_extra_decay,
        accepted, prior_step_states, output_norm_gain, output_projection,
    ) = args
    group_seqs, steps, feature_dev = tokens.shape
    own_seqs, _, heads, state_len = prior_step_states.shape
    own_rows = own_seqs * steps
    head_size = output_norm_gain.shape[0]
    inner = query_projection.shape[1]
    out_dev = output_projection.shape[1]
    rows = group_seqs * steps
    any_spec = pl.BlockSpec(memory_space=pl.ANY)
    vmem_spec = pl.BlockSpec(memory_space=pltpu.VMEM)
    dma = pltpu.SemaphoreType.DMA

    def hbm(array):
        return pltpu.with_memory_space_constraint(array, pltpu.HBM)

    mixed, states = pl.pallas_call(
        functools.partial(kernel, n, ntp, head_size),
        out_shape=(
            pltpu.VMEM((group_seqs, steps, out_dev), bf16),
            pltpu.VMEM(prior_step_states.shape, f32),
        ),
        in_specs=[any_spec] * 13,
        out_specs=(vmem_spec, vmem_spec),
        scratch_shapes=[
            pltpu.VMEM(tokens.shape, bf16),
            pltpu.VMEM((1, feature_dev), f32),
            pltpu.VMEM((3, feature_dev, inner), bf16),
            pltpu.VMEM((heads, feature_dev), bf16),
            pltpu.VMEM((heads, feature_dev), bf16),
            pltpu.VMEM((1, heads), f32),
            pltpu.VMEM(token_extra_decay.shape, f32),
            pltpu.SMEM(accepted.shape, jnp.int32),
            pltpu.VMEM(prior_step_states.shape, f32),
            pltpu.VMEM((1, head_size), f32),
            pltpu.VMEM((inner, out_dev), bf16),
            pltpu.VMEM((rows, feature_dev), f32),
            pltpu.VMEM((3, n, own_rows, inner), f32),
            pltpu.VMEM((n, own_rows, LANES), f32),
            pltpu.VMEM((n, 3, own_rows, inner), bf16),
            pltpu.VMEM((n - 1, 3, own_rows, inner), bf16),
            pltpu.VMEM((n - 1, own_rows, LANES), f32),
            pltpu.VMEM((3, own_rows, heads, head_size), f32),
            pltpu.VMEM((own_rows, LANES), f32),
            pltpu.VMEM((2 * head_size, state_len), bf16),
            pltpu.VMEM((2, own_rows * heads, state_len), f32),
            pltpu.VMEM((own_rows, heads, head_size), f32),
            pltpu.VMEM((own_rows, inner), f32),
            pltpu.VMEM((own_rows, inner), bf16),
            pltpu.VMEM((n - 1, own_rows, inner), bf16),
            pltpu.VMEM((n, own_rows, out_dev), bf16),
            pltpu.VMEM((ntp - 1, n, own_rows, out_dev), bf16),
            dma((13,)),
            dma((4, n - 1)),
            dma((4, n - 1)),
            dma((n - 1,)),
            dma((n - 1,)),
            dma((ntp - 1, n)),
            dma((ntp - 1, n)),
        ],
        compiler_params=pltpu.CompilerParams(
            collective_id=0, has_side_effects=True, vmem_limit_bytes=VMEM_LIMIT
        ),
    )(*map(hbm, (
        tokens, input_norm_gain.reshape(1, feature_dev), query_projection, key_projection,
        value_projection, write_strength_weight.T, decay_projection.T,
        head_decay_rate.reshape(1, heads), token_extra_decay, accepted, prior_step_states,
        output_norm_gain.reshape(1, head_size), output_projection,
    )))
    return pl.pallas_call(
        finish,
        out_shape=(
            jax.ShapeDtypeStruct(mixed.shape, bf16),
            jax.ShapeDtypeStruct(states.shape, f32),
        ),
        in_specs=[vmem_spec, vmem_spec],
        out_specs=(any_spec, any_spec),
        scratch_shapes=[dma((1 + own_rows,))],
        compiler_params=pltpu.CompilerParams(vmem_limit_bytes=VMEM_LIMIT // 4),
    )(mixed, states)


def solution(mesh):
    in_specs = (
        P("dp", None, "kv"),
        P("kv"),
        P("kv", "tp"),
        P("kv", "tp"),
        P("kv", "tp"),
        P("kv", "tp"),
        P("kv", "tp"),
        P("tp"),
        P(("dp", "kv"), None, "tp"),
        P(("dp", "kv")),
        P(("dp", "kv"), None, "tp", None),
        P(),
        P("tp", "kv"),
    )
    out_specs = (P("dp", None, "kv"), P(("dp", "kv"), None, "tp", None))
    body = functools.partial(per_device, mesh.shape["kv"], mesh.shape["tp"])
    return jax.shard_map(
        body, mesh=mesh, in_specs=in_specs, out_specs=out_specs, check_vma=False
    )
```

profile of v0, /device:TPU:0, one launch (start us, length us, event | category | flops | bytes accessed | tf_op | source)
XLA Modules:
  0.0 18.1 jit_solution(4904897217136821980)
XLA Ops:
  0.6 16.4 %shard_map.140 = (bf16[8,4,512]{2,1,0:T(4,128)(2,1)S(1)}, f32[2,4,8,4096]{3,2,1,0:T(8,128)S(1)}) custom-call(bf16[8,4,512]{2,1,0:T(4,128)(2,1)} %tokens_hbm.1, f32[1,512]{1,0:T(1,128)} %bitcast.7, bf16[512,512]{1,0:T(8,128)(2,1)} %wq_hbm.1, bf16[512,512]{1,0:T(8,128)(2,1)} %wk_hbm.1, bf16[512,512]{1,0:T(8,128)(2,1)} %wv_hbm.1, bf16[8,512]{1,0:T(8,128)(2,1)} %bitcast.5, ...), custom_call_target="tpu_custom_call" | custom-call | tf_op jit(solution)/shard_map/pallas_call | solution.py:335
  17.1 1.0 %shard_map.141 = (bf16[8,4,512]{2,1,0:T(4,128)(2,1)}, f32[2,4,8,4096]{3,2,1,0:T(8,128)}) custom-call(bf16[8,4,512]{2,1,0:T(4,128)(2,1)S(1)} %get-tuple-element.4.mixed_v, f32[2,4,8,4096]{3,2,1,0:T(8,128)S(1)} %get-tuple-element.5.states_v), custom_call_target="tpu_custom_call" | custom-call | tf_op jit(solution)/shard_map/pallas_call | solution.py:388
where the time goes:
time: 18.3 us; the launch traced here: 18.1 us
  Pallas kernels  17.5 us (96%)
  between operations  0.64 us (3%)
    pallas_call x1, Pallas kernels, per_device(): pl.pallas_call(functools.partial(kernel, n, ntp, head_size), out_shape=(p...  16.4 us
    pallas_call x1, Pallas kernels, per_device(): pl.pallas_call(finish, out_shape=(jax.ShapeDtypeStruct(mixed.shape, bf16)...  1.04 us

commit v1 on v0

v1 whole, which is shorter than its diff:
```python
import functools
import jax
import jax.numpy as jnp
from jax import lax
from jax.experimental import pallas as pl
from jax.experimental.pallas import tpu as pltpu
from jax.sharding import PartitionSpec as P

epsilon = 1e-06
MESH = pl.DeviceIdType.MESH
f32 = jnp.float32
bf16 = jnp.bfloat16
LANES = 128
VMEM_LIMIT = 32 * 2 ** 20


def silu(u):
    return u / (1.0 + jnp.exp(-u))


def wait_bytes(ref, sem):
    pltpu.make_async_copy(ref, ref, sem).wait()


def kernel(
    n,
    ntp,
    head_size,
    tokens_hbm,
    gain_hbm,
    wq_hbm,
    wk_hbm,
    wv_hbm,
    wb_hbm,
    wd_hbm,
    rate_hbm,
    extra_hbm,
    accepted_hbm,
    prior_hbm,
    onorm_hbm,
    wo_hbm,
    mixed_ref,
    states_v,
    tokens_v,
    gain_v,
    w_v,
    wbd_v,
    rate_v,
    extra_v,
    accepted_s,
    prior_v,
    onorm_v,
    wo_v,
    x_v,
    aux_v,
    send_v,
    recv_v,
    start_v,
    block_v,
    limits_v,
    spread_v,
    ones_v,
    tall_v,
    normed_v,
    recvn_v,
    parts_v,
    heads_v,
    expand_v,
    load_sem,
    regular_sem,
    send_sem,
    recv_sem,
):
    me = lax.axis_index("kv")
    my_tp = lax.axis_index("tp")
    root = ntp - 1
    is_root = my_tp == root
    group_seqs, steps, feature_dev = tokens_v.shape
    own_seqs, _, heads, state_len = prior_v.shape
    own_rows = own_seqs * steps
    model_width = n * feature_dev
    inner = heads * head_size
    pairs = inner // LANES
    blocks = ntp * pairs
    per_block = LANES // head_size
    RS, START, LIMITS, WO, GATHER, PARTS, GATHER_ROOT = range(7)
    here = regular_sem.at[0]

    def device(o, p):
        return {"kv": lax.rem(me + o, n), "tp": p}

    barrier = pltpu.get_barrier_semaphore()

    @pl.when(is_root)
    def _():
        for o in range(1, n):
            pl.semaphore_signal(
                barrier, inc=1, device_id=device(o, root), device_id_type=MESH
            )
        for p in range(root):
            for o in range(n):
                pl.semaphore_signal(
                    barrier, inc=1, device_id=device(o, p), device_id_type=MESH
                )

    loads = {}
    for index, (name, source, target) in enumerate((
        ("tokens", tokens_hbm, tokens_v),
        ("gain", gain_hbm, gain_v),
        ("wb", wb_hbm, wbd_v.at[0]),
        ("wd", wd_hbm, wbd_v.at[1]),
        ("q", wq_hbm, w_v.at[0]),
        ("k", wk_hbm, w_v.at[1]),
        ("v", wv_hbm, w_v.at[2]),
        ("prior", prior_hbm, prior_v),
        ("rate", rate_hbm, rate_v),
        ("extra", extra_hbm, extra_v),
        ("accepted", accepted_hbm, accepted_s),
        ("onorm", onorm_hbm, onorm_v),
        ("wo", wo_hbm, wo_v.at[my_tp]),
    )):
        loads[name] = pltpu.make_async_copy(source, target, load_sem.at[index])
        loads[name].start()

    loads["tokens"].wait()
    loads["gain"].wait()
    for s in range(group_seqs):
        x_v[s * steps:(s + 1) * steps, :] = tokens_v[s].astype(f32)
    x = x_v[...]
    squares = jnp.sum(x * x, axis=1, keepdims=True)
    scaled = (x * gain_v[...]).astype(bf16)

    contract_last = (((1,), (1,)), ((), ()))
    loads["wb"].wait()
    loads["wd"].wait()
    lane_x = lax.broadcasted_iota(jnp.int32, (x.shape[0], LANES), 1)
    half = LANES // 2
    aux_v[...] = jnp.where(lane_x >= half, squares, 0.0)
    for index in range(2):
        aux_v[:, index * heads:(index + 1) * heads] = lax.dot_general(
            scaled, wbd_v[index], contract_last, preferred_element_type=f32
        )
    send_v[:, :, 3 * inner:3 * inner + LANES] = (
        aux_v[...].reshape(n, own_rows, LANES).astype(bf16)
    )
    send_v[:, :, 3 * inner + LANES:] = (
        jnp.where(lane_x < half, squares, 0.0).reshape(n, own_rows, LANES).astype(bf16)
    )
    for piece, name in enumerate("qkv"):
        loads[name].wait()
        part = jnp.dot(scaled, w_v[piece], preferred_element_type=f32)
        send_v[:, :, piece * inner:(piece + 1) * inner] = (
            part.reshape(n, own_rows, inner).astype(bf16)
        )

    def remote(source, target, kind, where):
        pltpu.make_async_remote_copy(
            src_ref=source,
            dst_ref=target,
            send_sem=send_sem.at[kind],
            recv_sem=recv_sem.at[GATHER if kind == GATHER_ROOT else kind],
            device_id=where,
            device_id_type=MESH,
        ).start()

    @pl.when(is_root)
    def _():
        pl.semaphore_wait(barrier, n - 1)
        for o in range(1, n):
            remote(send_v.at[lax.rem(me + o, n)], recv_v.at[o - 1], RS, device(o, root))

    @pl.when(jnp.logical_not(is_root))
    def _():
        pl.semaphore_wait(barrier, n)
        for o in range(n):
            remote(
                send_v.at[lax.rem(me + o, n)], recv_v.at[n - 1 + my_tp * n + o], RS,
                device(o, root),
            )
        for o in range(n):
            pl.semaphore_signal(here, inc=1, device_id=device(o, root), device_id_type=MESH)

    for name in ("rate", "extra", "accepted", "onorm", "prior"):
        loads[name].wait()

    limits_v[my_tp] = jnp.zeros(limits_v.shape[1:], f32)
    limits_v[my_tp, 0, :, heads:2 * heads] = jnp.broadcast_to(rate_v[...], (own_rows, heads))
    for s in range(own_seqs):
        limits_v[my_tp, 1, s * steps:(s + 1) * steps, heads:2 * heads] = extra_v[s]

    lane = lax.broadcasted_iota(jnp.int32, (heads, LANES), 1)
    head = lax.broadcasted_iota(jnp.int32, (heads, LANES), 0)
    first_half = lane < head_size
    even_head = lax.rem(head, 2) == 0
    diagonal = first_half == even_head
    for s in range(own_seqs):
        state = prior_v[s, jnp.clip(accepted_s[s] - 1, 0, steps - 1)]
        for j in range(state_len // LANES):
            both = state[:, j * LANES:(j + 1) * LANES]
            turned = pltpu.roll(both, head_size, 1)
            for half_index, right_lanes in ((0, even_head), (1, jnp.logical_not(even_head))):
                rows = jnp.where(diagonal, jnp.where(right_lanes, both, turned), 0.0)
                start_v[s, pl.ds(2 * j + half_index, heads, stride=head_size), :] = rows
        block_v[my_tp, :, s * LANES:(s + 1) * LANES] = start_v[s].astype(bf16)

    @pl.when(jnp.logical_not(is_root))
    def _():
        remote(block_v.at[my_tp], block_v.at[my_tp], START, device(0, root))
        remote(limits_v.at[my_tp], limits_v.at[my_tp], LIMITS, device(0, root))

    loads["wo"].wait()

    @pl.when(jnp.logical_not(is_root))
    def _():
        remote(wo_v.at[my_tp], wo_v.at[my_tp], WO, device(0, root))

    @pl.when(is_root)
    def _():
        pl.semaphore_wait(here, n * root)
        for p in range(root):
            remote(wo_v.at[my_tp], wo_v.at[my_tp], WO, device(0, p))

    entry = lax.broadcasted_iota(jnp.int32, spread_v.shape, 0)
    column = lax.broadcasted_iota(jnp.int32, spread_v.shape, 1)
    first = jnp.where(entry < head_size, entry, entry - head_size) * head_size
    spread_v[...] = jnp.where(
        (column >= first) & (column < first + head_size), 1.0, 0.0
    ).astype(bf16)
    entry = lax.broadcasted_iota(jnp.int32, ones_v.shape, 0)
    column = lax.broadcasted_iota(jnp.int32, ones_v.shape, 1)
    ones_v[...] = jnp.where(
        (entry < head_size) == (column < head_size), 1.0, 0.0
    ).astype(bf16)

    Q, K, V, QS, KS, BETA, DECAY = range(7)

    def tall(item, s, t):
        row = (s * steps + t) * blocks
        return tall_v[item, row:row + blocks, :]

    def heads_of(p):
        for item in range(3):
            for pair in range(pairs):
                value = parts_v[item, pl.ds(p * pairs + pair, own_rows, stride=blocks), :]
                turned = pltpu.roll(value, head_size, 1)
                left = lax.broadcasted_iota(jnp.int32, value.shape, 1) < head_size
                for sub, (one, two) in enumerate(((value, turned), (turned, value))):
                    heads_v[item, pl.ds(pair * per_block + sub, own_rows, stride=heads), :] = (
                        jnp.where(left, one, two)
                    )

    @pl.when(is_root)
    def _():
        row_lane = lax.broadcasted_iota(jnp.int32, (own_rows, LANES), 1)
        row_first = row_lane < head_size
        row_seq = lax.broadcasted_iota(jnp.int32, (2 * own_rows, LANES), 0)
        row_seq = lax.rem(row_seq, own_rows)
        wait_bytes(recv_v, recv_sem.at[RS])
        for p in range(root):
            wait_bytes(block_v.at[p], recv_sem.at[START])
            wait_bytes(limits_v.at[p], recv_sem.at[LIMITS])
        for p in range(ntp):
            if p == root:
                parts = [send_v[me].astype(f32)]
                parts += [recv_v[o - 1].astype(f32) for o in range(1, n)]
            else:
                parts = [recv_v[n - 1 + p * n + o].astype(f32) for o in range(n)]
            total = functools.reduce(jnp.add, parts)
            low_block = total[:, 3 * inner:3 * inner + LANES]
            high_block = total[:, 3 * inner + LANES:]
            inverse = lax.rsqrt(
                jnp.where(row_lane < half, high_block, low_block) / model_width + epsilon
            )
            gates = low_block * inverse
            beta = 1.0 / (1.0 + jnp.exp(-gates))
            softplus = jnp.maximum(gates, 0.0) + jnp.log1p(jnp.exp(-jnp.abs(gates)))
            decay = jnp.exp(limits_v[p, 1] - limits_v[p, 0] * softplus)
            for pair in range(pairs):
                block = p * pairs + pair
                rows = pl.ds(block, own_rows, stride=blocks)
                values = [
                    silu(
                        total[:, c * inner + pair * LANES:c * inner + (pair + 1) * LANES]
                        * inverse
                    )
                    for c in range(3)
                ]
                for item in (Q, K, V):
                    tall_v[item, rows, :] = values[item]
                both = jnp.concatenate([values[Q], values[K]], axis=0).astype(bf16)
                product = jnp.dot(
                    both, block_v[p, pair * LANES:(pair + 1) * LANES, :],
                    preferred_element_type=f32,
                )
                chosen = product[:, 0:LANES]
                for s in range(1, own_seqs):
                    chosen = jnp.where(
                        row_seq >= s * steps, product[:, s * LANES:(s + 1) * LANES], chosen
                    )
                tall_v[QS, rows, :] = chosen[:own_rows]
                tall_v[KS, rows, :] = chosen[own_rows:]
                for item, gate, offset in ((BETA, beta, 0), (DECAY, decay, heads)):
                    place = offset + pair * per_block
                    tall_v[item, rows, :] = jnp.where(
                        row_first, gate[:, place:place + 1], gate[:, place + 1:place + 2]
                    )

        products = []
        for s in range(own_seqs):
            for t in range(steps):
                query, key = tall(Q, s, t), tall(K, s, t)
                products += [query * query, key * key]
                for j in range(t):
                    products += [key * tall(K, s, j), query * tall(K, s, j)]
                products.append(query * key)
        products = jnp.concatenate(products, axis=0).astype(bf16)
        sums = jnp.dot(products, ones_v[...], preferred_element_type=f32)
        sums = iter([sums[i * blocks:(i + 1) * blocks] for i in range(sums.shape[0] // blocks)])
        attended = []
        writes = []
        keys = []
        for s in range(own_seqs):
            query_scale, key_scale, key_dots, query_dots = [], [], {}, {}
            for t in range(steps):
                query_scale.append(lax.rsqrt(next(sums) + epsilon) * head_size ** -0.5)
                key_scale.append(lax.rsqrt(next(sums) + epsilon))
                for j in range(t):
                    key_dots[t, j] = next(sums) * (key_scale[t] * key_scale[j])
                    query_dots[t, j] = next(sums) * (query_scale[t] * key_scale[j])
                query_dots[t, t] = next(sums) * (query_scale[t] * key_scale[t])
            write = []
            grown = None
            spans = []
            for t in range(steps):
                decay, beta = tall(DECAY, s, t), tall(BETA, s, t)
                grown = decay if t == 0 else grown * decay
                spans = [span * decay for span in spans]
                held = grown * key_scale[t] * tall(KS, s, t)
                seen = grown * query_scale[t] * tall(QS, s, t)
                for j in range(t):
                    held = held + spans[j] * key_dots[t, j] * write[j]
                    seen = seen + spans[j] * query_dots[t, j] * write[j]
                write.append(beta * (tall(V, s, t) - held))
                spans.append(jnp.ones_like(decay))
                attended.append(seen + query_dots[t, t] * write[t])
            writes += write
            keys += key_scale
        squared = jnp.concatenate([a * a for a in attended], axis=0).astype(bf16)
        means = jnp.dot(squared, ones_v[...], preferred_element_type=f32) / head_size
        norm_gain = jnp.concatenate([onorm_v[...]] * per_block, axis=1)
        for row in range(own_rows):
            scale = lax.rsqrt(means[row * blocks:(row + 1) * blocks] + epsilon)
            normed_v[row * blocks:(row + 1) * blocks, :] = attended[row] * scale * norm_gain
        for block in range(blocks):
            recvn_v[me, :, block * LANES:(block + 1) * LANES] = (
                normed_v[pl.ds(block, own_rows, stride=blocks), :].astype(bf16)
            )
        for o in range(1, n):
            remote(recvn_v.at[me], recvn_v.at[me], GATHER_ROOT, device(o, root))
        for p in range(root):
            for o in range(n):
                remote(recvn_v.at[me], recvn_v.at[me], GATHER, device(o, p))
        for s in range(own_seqs):
            for t in range(steps):
                row = s * steps + t
                rows = slice(row * blocks, (row + 1) * blocks)
                parts_v[0, rows, :] = tall(K, s, t) * keys[row]
                parts_v[1, rows, :] = writes[row]
                parts_v[2, rows, :] = tall(DECAY, s, t)
        for p in range(root):
            remote(parts_v, parts_v, PARTS, device(0, p))
        heads_of(root)

    @pl.when(jnp.logical_not(is_root))
    def _():
        wait_bytes(parts_v, recv_sem.at[PARTS])
        for p in range(root):
            @pl.when(my_tp == p)
            def _():
                heads_of(p)

    keys = heads_v[0, :, 0:head_size]
    high = keys.astype(bf16)
    low = (keys - high.astype(f32)).astype(bf16)
    both = jnp.concatenate([high.astype(f32), low.astype(f32)], axis=1).astype(bf16)
    expand_v[...] = jnp.dot(both, spread_v[...], preferred_element_type=f32)

    def wide(value):
        return jnp.concatenate([value] * (state_len // LANES), axis=1)

    for s in range(own_seqs):
        state = prior_v[s, jnp.clip(accepted_s[s] - 1, 0, steps - 1)]
        for t in range(steps):
            block = slice((s * steps + t) * heads, (s * steps + t + 1) * heads)
            state = wide(heads_v[2, block, :]) * state + (
                expand_v[block, :] * wide(heads_v[1, block, :])
            )
            states_v[s, t] = state

    for p in range(root):
        wait_bytes(wo_v.at[p], recv_sem.at[WO])

    @pl.when(is_root)
    def _():
        wait_bytes(recvn_v.at[pl.ds(0, n - 1)], recv_sem.at[GATHER])

    @pl.when(jnp.logical_not(is_root))
    def _():
        wait_bytes(recvn_v, recv_sem.at[GATHER])

    rows = recvn_v[...].reshape(n * own_rows, ntp * inner)
    weights = wo_v[...].reshape(ntp * inner, wo_v.shape[2])
    mixed = jnp.dot(rows, weights, preferred_element_type=f32)
    for s in range(group_seqs):
        mixed_ref[s] = mixed[s * steps:(s + 1) * steps].astype(bf16)

    for p in range(root):
        wait_bytes(wo_v.at[p], send_sem.at[WO])

    @pl.when(is_root)
    def _():
        wait_bytes(send_v.at[pl.ds(0, n - 1)], send_sem.at[RS])
        wait_bytes(recvn_v.at[pl.ds(0, n - 1)], send_sem.at[GATHER_ROOT])
        for p in range(root):
            wait_bytes(recvn_v, send_sem.at[GATHER])
            wait_bytes(parts_v, send_sem.at[PARTS])

    @pl.when(jnp.logical_not(is_root))
    def _():
        wait_bytes(send_v, send_sem.at[RS])
        wait_bytes(block_v.at[0], send_sem.at[START])
        wait_bytes(limits_v.at[0], send_sem.at[LIMITS])


def finish(mixed_v, states_v, mixed_hbm, states_hbm, sem):
    own_seqs, steps = states_v.shape[:2]
    copies = [
        pltpu.make_async_copy(
            states_v.at[s, t], states_hbm.at[s, t], sem.at[1 + s * steps + t]
        )
        for s in range(own_seqs)
        for t in range(steps)
    ]
    copies.append(pltpu.make_async_copy(mixed_v, mixed_hbm, sem.at[0]))
    for copy in copies:
        copy.start()
    for copy in copies:
        copy.wait()


def per_device(n, ntp, *args):
    (
        tokens, input_norm_gain, query_projection, key_projection, value_projection,
        write_strength_weight, decay_projection, head_decay_rate, token_extra_decay,
        accepted, prior_step_states, output_norm_gain, output_projection,
    ) = args
    group_seqs, steps, feature_dev = tokens.shape
    own_seqs, _, heads, state_len = prior_step_states.shape
    own_rows = own_seqs * steps
    head_size = output_norm_gain.shape[0]
    inner = query_projection.shape[1]
    out_dev = output_projection.shape[1]
    rows = group_seqs * steps
    pairs = inner // LANES
    blocks = ntp * pairs
    width = 3 * inner + 2 * LANES
    any_spec = pl.BlockSpec(memory_space=pl.ANY)
    vmem_spec = pl.BlockSpec(memory_space=pltpu.VMEM)
    dma = pltpu.SemaphoreType.DMA

    def hbm(array):
        return pltpu.with_memory_space_constraint(array, pltpu.HBM)

    mixed, states = pl.pallas_call(
        functools.partial(kernel, n, ntp, head_size),
        out_shape=(
            pltpu.VMEM((group_seqs, steps, out_dev), bf16),
            pltpu.VMEM(prior_step_states.shape, f32),
        ),
        in_specs=[any_spec] * 13,
        out_specs=(vmem_spec, vmem_spec),
        scratch_shapes=[
            pltpu.VMEM(tokens.shape, bf16),
            pltpu.VMEM((1, feature_dev), f32),
            pltpu.VMEM((3, feature_dev, inner), bf16),
            pltpu.VMEM((2, heads, feature_dev), bf16),
            pltpu.VMEM((1, heads), f32),
            pltpu.VMEM(token_extra_decay.shape, f32),
            pltpu.SMEM(accepted.shape, jnp.int32),
            pltpu.VMEM(prior_step_states.shape, f32),
            pltpu.VMEM((1, head_size), f32),
            pltpu.VMEM((ntp, inner, out_dev), bf16),
            pltpu.VMEM((rows, feature_dev), f32),
            pltpu.VMEM((rows, LANES), f32),
            pltpu.VMEM((n, own_rows, width), bf16),
            pltpu.VMEM((ntp * n - 1, own_rows, width), bf16),
            pltpu.VMEM((own_seqs, inner, LANES), f32),
            pltpu.VMEM((ntp, inner, own_seqs * LANES), bf16),
            pltpu.VMEM((ntp, 2, own_rows, LANES), f32),
            pltpu.VMEM((2 * head_size, state_len), bf16),
            pltpu.VMEM((LANES, LANES), bf16),
            pltpu.VMEM((7, own_rows * blocks, LANES), f32),
            pltpu.VMEM((own_rows * blocks, LANES), f32),
            pltpu.VMEM((n, own_rows, ntp * inner), bf16),
            pltpu.VMEM((3, own_rows * blocks, LANES), f32),
            pltpu.VMEM((3, own_rows * heads, LANES), f32),
            pltpu.VMEM((own_rows * heads, state_len), f32),
            dma((13,)),
            pltpu.SemaphoreType.REGULAR((1,)),
            dma((7,)),
            dma((6,)),
        ],
        compiler_params=pltpu.CompilerParams(
            collective_id=0, has_side_effects=True, vmem_limit_bytes=VMEM_LIMIT
        ),
    )(*map(hbm, (
        tokens, input_norm_gain.reshape(1, feature_dev), query_projection, key_projection,
        value_projection, write_strength_weight.T, decay_projection.T,
        head_decay_rate.reshape(1, heads), token_extra_decay, accepted, prior_step_states,
        output_norm_gain.reshape(1, head_size), output_projection,
    )))
    return pl.pallas_call(
        finish,
        out_shape=(
            jax.ShapeDtypeStruct(mixed.shape, bf16),
            jax.ShapeDtypeStruct(states.shape, f32),
        ),
        in_specs=[vmem_spec, vmem_spec],
        out_specs=(any_spec, any_spec),
        scratch_shapes=[dma((1 + own_rows,))],
        compiler_params=pltpu.CompilerParams(vmem_limit_bytes=VMEM_LIMIT // 4),
    )(mixed, states)


def solution(mesh):
    in_specs = (
        P("dp", None, "kv"),
        P("kv"),
        P("kv", "tp"),
        P("kv", "tp"),
        P("kv", "tp"),
        P("kv", "tp"),
        P("kv", "tp"),
        P("tp"),
        P(("dp", "kv"), None, "tp"),
        P(("dp", "kv")),
        P(("dp", "kv"), None, "tp", None),
        P(),
        P("tp", "kv"),
    )
    out_specs = (P("dp", None, "kv"), P(("dp", "kv"), None, "tp", None))
    body = functools.partial(per_device, mesh.shape["kv"], mesh.shape["tp"])
    return jax.shard_map(
        body, mesh=mesh, in_specs=in_specs, out_specs=out_specs, check_vma=False
    )
```

time: 18.3 us -> 15.4 us (0.84)
  Pallas kernels: 17.5 us -> 14.6 us
    pallas_call x1, Pallas kernels: 16.4 us -> 13.5 us  [per_device(): pl.pallas_call(functools.partial(kernel, n, ntp, head_size), out_shape=(p...]
where the time goes in v1:
time: 15.4 us; the launch traced here: 15.2 us
  Pallas kernels  14.6 us (95%)
  between operations  0.64 us (4%)
    pallas_call x1, Pallas kernels, per_device(): pl.pallas_call(functools.partial(kernel, n, ntp, head_size), out_shape=(p...  13.5 us
    pallas_call x1, Pallas kernels, per_device(): pl.pallas_call(finish, out_shape=(jax.ShapeDtypeStruct(mixed.shape, bf16)...  1.04 us

profile of v1, /device:TPU:0, one launch (start us, length us, event | category | flops | bytes accessed | tf_op | source)
XLA Modules:
  0.0 15.2 jit_solution(1107085140853729251)
XLA Ops:
  0.6 13.5 %shard_map.140 = (bf16[8,4,512]{2,1,0:T(4,128)(2,1)S(1)}, f32[2,4,8,4096]{3,2,1,0:T(8,128)S(1)}) custom-call(bf16[8,4,512]{2,1,0:T(4,128)(2,1)} %tokens_hbm.1, f32[1,512]{1,0:T(1,128)} %bitcast.7, bf16[512,512]{1,0:T(8,128)(2,1)} %wq_hbm.1, bf16[512,512]{1,0:T(8,128)(2,1)} %wk_hbm.1, bf16[512,512]{1,0:T(8,128)(2,1)} %wv_hbm.1, bf16[8,512]{1,0:T(8,128)(2,1)} %bitcast.5, ...), custom_call_target="tpu_custom_call" | custom-call | tf_op jit(solution)/shard_map/pallas_call | solution.py:474
  14.2 1.0 %shard_map.141 = (bf16[8,4,512]{2,1,0:T(4,128)(2,1)}, f32[2,4,8,4096]{3,2,1,0:T(8,128)}) custom-call(bf16[8,4,512]{2,1,0:T(4,128)(2,1)S(1)} %get-tuple-element.4.mixed_v, f32[2,4,8,4096]{3,2,1,0:T(8,128)S(1)} %get-tuple-element.5.states_v), custom_call_target="tpu_custom_call" | custom-call | tf_op jit(solution)/shard_map/pallas_call | solution.py:522
